TPU v7x, 128 devices: a whole 4x4x4 slice. The times are simulated.
128 devices in a mesh: ep: 64 (over z, y, x), tp: 2 (over core).
Axes of the slice: x: 4, y: 4, z: 4, core: 2. Of those that a mesh axis runs over, the one named last changes fastest.
Arguments:
- tokens: bfloat16 [256, 1024], P('ep'), may hold values from -6 to 6
- mixer_gain: float32 [1024], replicated, may hold values from 0.1 to 1.9
- w_query: bfloat16 [1024, 2048], P(None, 'tp'), may hold values from -0.1875 to 0.1875
- w_key: bfloat16 [1024, 2048], P(None, 'tp'), may hold values from -0.1875 to 0.1875
- w_value: bfloat16 [1024, 2048], P(None, 'tp'), may hold values from -0.1875 to 0.1875
- w_input_gate: bfloat16 [1024, 4], P(None, 'tp'), may hold values from -0.1875 to 0.1875
- w_forget_gate: bfloat16 [1024, 4], P(None, 'tp'), may hold values from -0.1875 to 0.1875
- forget_bias: float32 [4], P('tp'), may hold values from -1 to 3
- w_output: bfloat16 [2048, 1024], P('tp'), may hold values from -0.125 to 0.125
- memory: float32 [256, 4, 512, 512], P('ep', 'tp'), may hold values from -0.26516503 to 0.26516503
- normalizer: float32 [256, 4, 512], P('ep', 'tp'), may hold values from -0.26516503 to 0.26516503
- stabilizer: float32 [256, 4], P('ep', 'tp'), may hold values from -2 to 2
- ffn_gain: float32 [1024], replicated, may hold values from 0.1 to 1.9
- route_ids: int32 [256, 2], P('ep'), may hold values from 0 to 7, all different within a row; in each aligned block of 4 rows (0 to 3, 4 to 7, ...) at most 2 rows name the same one
- route_weights: float32 [256, 2], P('ep'), may hold values from 0.1 to 1
- expert_gate: bfloat16 [64, 1024, 704], P('ep', None, 'tp'), may hold values from -0.1875 to 0.1875
- expert_up: bfloat16 [64, 1024, 704], P('ep', None, 'tp'), may hold values from -0.1875 to 0.1875
- expert_down: bfloat16 [64, 704, 1024], P('ep', 'tp'), may hold values from -0.078125 to 0.078125
- dense_gate_w: bfloat16 [1024, 4096], P(None, ('ep', 'tp')), may hold values from -0.1875 to 0.1875
- dense_up_w: bfloat16 [1024, 4096], P(None, ('ep', 'tp')), may hold values from -0.1875 to 0.1875
- dense_down_w: bfloat16 [4096, 1024], P(('ep', 'tp')), may hold values from -0.09375 to 0.09375
- dense_scale: float32 [1024], P('tp'), may hold values from 0.3 to 1.5
Outputs:
- output: bfloat16 [256, 1024], P('ep', 'tp')
- new_memory: float32 [256, 4, 512, 512], P('ep', 'tp')
- new_normalizer: float32 [256, 4, 512], P('ep', 'tp')
- new_stabilizer: float32 [256, 4], P('ep', 'tp')
Inputs may be any that keep to these rules, and one draw needn't show every extreme that they name: `route_ids`: the two experts of a row differ. In each aligned block of 4 rows (the rows of one device group) no expert is named by more than 2 rows, a bound that some block reaches.
All inputs are finite; a program needn't handle non-finite values.
Results may differ from a plain program's by a relative error of at most 0.015.
Values may be sent and summed in bfloat16 or wider, within the bound.
A program may use at most 128 MiB of HBM per device.

v0:
```python
import jax
import jax.numpy as jnp
from jax import lax
from jax.sharding import PartitionSpec as P

EXPERTS = 8
CAPACITY = 2


epsilon = 1e-06


def over_pieces(shard, axis):
    return lax.all_gather(shard, axis).astype(jnp.float32).sum(0)


def copy_for_each(shard, axis):
    copies = jnp.broadcast_to(shard, (lax.axis_size(axis), *shard.shape))
    return lax.all_to_all(copies, axis, split_axis=0, concat_axis=0, tiled=True)


def in_order(blocks, dim):
    shape = list(blocks.shape[1:])
    shape[dim] *= blocks.shape[0]
    return jnp.moveaxis(blocks, 0, dim).reshape(shape)


def gather_directly(shard, axis, dim):
    blocks = copy_for_each(shard, axis)
    return in_order(blocks, dim)


def cut_along(shard, dim, length):
    shape = shard.shape
    blocks = shard.reshape(*shape[:dim], length, shape[dim] // length, *shape[dim + 1 :])
    return jnp.moveaxis(blocks, dim, 0)


def sent_and_summed(shard, axis, dim):
    blocks = cut_along(shard, dim, lax.axis_size(axis))
    arrived = lax.all_to_all(blocks, axis, split_axis=0, concat_axis=0, tiled=True)
    return arrived.astype(jnp.float32).sum(axis=0)


def sent_together(arrays, axis, dim, along):
    ends, at = ([], 0)
    for a in arrays[:-1]:
        at += a.shape[along]
        ends.append(at)
    both = jnp.concatenate(arrays, axis=along)
    return tuple(jnp.split(sent_and_summed(both, axis, dim), ends, axis=along))


def normalize(values_in, gain):
    values = values_in.astype(jnp.float32)
    scale = lax.rsqrt(jnp.mean(values * values, axis=-1, keepdims=True) + epsilon)
    return (values * scale * gain).astype(jnp.bfloat16)


def cell_step(
    query_heads, key_heads, value_heads, in_gate, forget_log, memory, normalizer, stabilizer
):
    new_stabilizer = jnp.maximum(forget_log + stabilizer, in_gate)
    carry = jnp.exp(forget_log + stabilizer - new_stabilizer)
    admit = jnp.exp(in_gate - new_stabilizer)
    scaled_key = admit[..., None] * key_heads
    new_memory = (
        carry[..., None, None] * memory + scaled_key[..., :, None] * value_heads[..., None, :]
    )
    new_normalizer = carry[..., None] * normalizer + scaled_key
    numer = jnp.einsum(
        "...hd,...hde->...he", query_heads, new_memory, precision=lax.Precision.HIGHEST
    )
    denom = jnp.sum(new_normalizer * query_heads, axis=-1)
    bound = jnp.maximum(jnp.abs(denom), jnp.exp(-new_stabilizer))
    return (numer / bound[..., None], new_memory, new_normalizer, new_stabilizer)


def shards(
    tokens,
    mixer_gain,
    w_query,
    w_key,
    w_value,
    w_input_gate,
    w_forget_gate,
    forget_bias,
    w_output,
    memory,
    normalizer,
    stabilizer,
    ffn_gain,
    route_ids,
    route_weights,
    expert_gate,
    expert_up,
    expert_down,
    dense_gate_w,
    dense_up_w,
    dense_down_w,
    dense_scale,
):
    local_rows = tokens.shape[0]
    local_heads = memory.shape[1]
    head_size = memory.shape[2]
    width = tokens.shape[1]
    normed = normalize(tokens, mixer_gain)
    query = jnp.dot(normed, w_query, preferred_element_type=jnp.float32).astype(jnp.bfloat16)
    key = jnp.dot(normed, w_key, preferred_element_type=jnp.float32).astype(jnp.bfloat16)
    value = jnp.dot(normed, w_value, preferred_element_type=jnp.float32).astype(jnp.bfloat16)
    in_gate = jnp.dot(normed, w_input_gate, preferred_element_type=jnp.float32)
    forget_log = jax.nn.log_sigmoid(
        jnp.dot(normed, w_forget_gate, preferred_element_type=jnp.float32) + forget_bias
    )
    shaped = (local_rows, local_heads, head_size)
    query_heads = query.astype(jnp.float32).reshape(shaped)
    key_heads = key.astype(jnp.float32).reshape(shaped) * head_size ** (-0.5)
    value_heads = value.astype(jnp.float32).reshape(shaped)
    read, new_memory, new_normalizer, new_stabilizer = cell_step(
        query_heads, key_heads, value_heads, in_gate, forget_log, memory, normalizer, stabilizer
    )
    read = read.reshape(local_rows, local_heads * head_size).astype(jnp.bfloat16)
    partial_value = jnp.dot(read, w_output, preferred_element_type=jnp.float32)
    mixed = over_pieces(partial_value.astype(jnp.bfloat16), "tp").astype(jnp.float32)
    stream = tokens.astype(jnp.float32) + mixed
    ffn_in = normalize(stream, ffn_gain)
    spread = lax.axis_size("ep") // EXPERTS
    chosen = (route_ids[:, :, None] == jnp.arange(EXPERTS, dtype=jnp.int32)[None, None, :]).astype(
        jnp.int32
    )
    choices_count = route_ids.shape[1]
    flat = chosen.reshape(local_rows * choices_count, EXPERTS)
    before = jnp.cumsum(flat, axis=0) - flat
    position = jnp.sum(before * flat, axis=1)
    placed = (position[:, None] == jnp.arange(CAPACITY, dtype=jnp.int32)[None, :]).astype(
        jnp.float32
    )
    table = (flat.astype(jnp.float32)[:, :, None] * placed[:, None, :]).reshape(
        local_rows, choices_count, EXPERTS, CAPACITY
    )
    member = jnp.sum(table, axis=1)
    combine = jnp.einsum("bk,bkec->bec", route_weights, table, precision=lax.Precision.HIGHEST)
    slot_rows = jnp.einsum(
        "bec,bd->ecd", member.astype(jnp.bfloat16), ffn_in, preferred_element_type=jnp.float32
    ).astype(jnp.bfloat16)
    outgoing = jnp.repeat(slot_rows, spread, axis=0).reshape(EXPERTS * spread * CAPACITY, width)
    incoming = lax.all_to_all(outgoing, "ep", split_axis=0, concat_axis=0, tiled=True)
    expert_gated = jnp.dot(incoming, expert_gate[0], preferred_element_type=jnp.float32)
    expert_lifted = jnp.dot(incoming, expert_up[0], preferred_element_type=jnp.float32)
    expert_hidden = (jax.nn.silu(expert_gated) * expert_lifted).astype(jnp.bfloat16)
    expert_part = jnp.dot(expert_hidden, expert_down[0], preferred_element_type=jnp.float32)
    gathered = gather_directly(ffn_in, "ep", 0)
    gated = jnp.dot(gathered, dense_gate_w, preferred_element_type=jnp.float32)
    lifted = jnp.dot(gathered, dense_up_w, preferred_element_type=jnp.float32)
    hidden = (jax.nn.silu(gated) * lifted).astype(jnp.bfloat16)
    dense_part = sent_and_summed(
        jnp.dot(hidden, dense_down_w, preferred_element_type=jnp.float32).astype(jnp.bfloat16),
        "ep",
        0,
    )
    expert_half, dense_half = sent_together(
        (expert_part.astype(jnp.bfloat16), dense_part.astype(jnp.bfloat16)), "tp", 1, 0
    )
    returned = lax.all_to_all(
        expert_half.astype(jnp.bfloat16), "ep", split_axis=0, concat_axis=0, tiled=True
    ).astype(expert_half.dtype)
    half_width = dense_half.shape[1]
    per_expert = jnp.sum(returned.reshape(EXPERTS, spread, CAPACITY, half_width), axis=1)
    routed = jnp.einsum("bec,ecd->bd", combine, per_expert, precision=lax.Precision.HIGHEST)
    column_start = lax.axis_index("tp") * half_width
    stream_half = lax.dynamic_slice_in_dim(stream, column_start, half_width, 1)
    output = (stream_half + routed + dense_scale * dense_half).astype(jnp.bfloat16)
    return (output, new_memory, new_normalizer, new_stabilizer)


def solution(mesh):
    placed = (
        P("ep", None),
        P(),
        P(None, "tp"),
        P(None, "tp"),
        P(None, "tp"),
        P(None, "tp"),
        P(None, "tp"),
        P("tp"),
        P("tp", None),
        P("ep", "tp", None, None),
        P("ep", "tp", None),
        P("ep", "tp"),
        P(),
        P("ep", None),
        P("ep", None),
        P("ep", None, "tp"),
        P("ep", None, "tp"),
        P("ep", "tp", None),
        P(None, ("ep", "tp")),
        P(None, ("ep", "tp")),
        P(("ep", "tp"), None),
        P("tp"),
    )
    return jax.shard_map(
        shards,
        mesh=mesh,
        in_specs=placed,
        out_specs=(P("ep", "tp"), P("ep", "tp", None, None), P("ep", "tp", None), P("ep", "tp")),
        check_vma=False,
    )
```

profile of v0, /device:TPU:0, one launch (start us, length us, event | category | flops | bytes accessed | tf_op | source)
XLA Modules:
  0.0 100.8 jit_solution(16225650972744075817)
XLA Ops:
  0.7 1.0 fusion.26
  1.7 0.8 fusion.28
  3.4 2.0 %fusion.3 = f32[4,1024]{1,0:T(4,128)S(1)} fusion(bf16[4,1024]{1,0:T(4,128)(2,1)S(1)} %fusion.28, bf16[1024,1024]{1,0:T(8,128)(2,1)} %param.25), kind=kOutput, calls=%fused_computation.12 | convolution fusion | flops 8396800 | bytes 2121728 | tf_op jit(solution)/shard_map/dot_general | solution.py:109
  5.6 0.7 multiply_reduce_fusion.1
  6.4 2.0 %fusion.2 = f32[4,1024]{1,0:T(4,128)S(1)} fusion(bf16[4,1024]{1,0:T(4,128)(2,1)S(1)} %fusion.28, bf16[1024,1024]{1,0:T(8,128)(2,1)} %param.26), kind=kOutput, calls=%fused_computation.10 | convolution fusion | flops 8396800 | bytes 2121728 | tf_op jit(solution)/shard_map/dot_general | solution.py:110
  8.5 4.0 %multiply_add_fusion = f32[4,2,512,512]{3,2,1,0:T(8,128)S(1)} fusion(f32[4,2,512,512]{3,2,1,0:T(8,128)} %param.31, f32[4,2,512]{2,1,0:T(2,128)S(1)} %reshape.129, f32[4,2,512]{2,1,0:T(2,128)S(1)} %get-tuple-element.8, f32[4,2]{1,0:T(4,128)S(1)} %copy.50), kind=kLoop, calls=%fused_computation | loop fusion | flops 6291456 | bytes 16810016 | tf_op jit(solution)/shard_map/add | solution.py:68
  12.5 2.9 %fusion.45 = f32[4,2,1,512]{3,2,1,0:T(1,128)S(1)} fusion(bf16[4,2,512,1]{2,3,1,0:T(2,128)(2,1)S(1)} %reshape.144, f32[4,2,512,512]{3,2,1,0:T(8,128)S(1)} %multiply_add_fusion), kind=kOutput, calls=%fused_computation.84 | convolution fusion | flops 25165824 | bytes 8413184 | tf_op jit(solution)/shard_map/...hd,...hde->...he/dot_general | solution.py:71
  15.4 0.6 copy-done.1
  16.6 1.8 %all-gather.1 = bf16[2,4,1024]{2,1,0:T(4,128)(2,1)S(1)} all-gather(bf16[1,4,1024]{2,1,0:T(4,128)(2,1)S(1)} %fusion.4), channel_id=2, replica_groups=mesh['ep'=64,'tp'=2] {'tp'}, dimensions={0}, use_global_device_ids=true | all-gather | bytes 24576 | tf_op jit(solution)/shard_map/all_gather | solution.py:14
  19.6 22.3 %all_to_all.36 = bf16[64,2,1024]{2,1,0:T(2,128)(2,1)S(1)} all-to-all(bf16[64,2,1024]{2,1,0:T(2,128)(2,1)S(1)} %bitcast.67), channel_id=1, replica_groups=mesh['ep'=64,'tp'=2] {'ep'}, dimensions={0} | all-to-all | bytes 524288 | tf_op jit(solution)/shard_map/all_to_all | solution.py:147
  41.9 0.9 broadcast_in_dim.5
  42.8 4.9 %all-to-all-start.1 = ((bf16[64,4,1024]{2,1,0:T(4,128)(2,1)}), bf16[64,4,1024]{2,1,0:T(4,128)(2,1)S(1)}, u32[]{:S(2)}, u32[]{:S(2)}) async-start(bf16[64,4,1024]{2,1,0:T(4,128)(2,1)} %broadcast_in_dim.5), calls=%async_computation.1 | async-start | bytes 1048576 | tf_op jit(solution)/shard_map/all_to_all | solution.py:19
  47.9 12.3 %all-to-all-done.1 = bf16[64,4,1024]{2,1,0:T(4,128)(2,1)S(1)} async-done(((bf16[64,4,1024]{2,1,0:T(4,128)(2,1)}), bf16[64,4,1024]{2,1,0:T(4,128)(2,1)S(1)}, u32[]{:S(2)}, u32[]{:S(2)}) %all-to-all-start.1) | async-done | bytes 524320 | tf_op jit(solution)/shard_map/all_to_all | solution.py:19
  60.6 1.7 %convolution_convert_fusion = bf16[256,1024]{1,0:T(8,128)(2,1)S(1)} fusion(bf16[32,1024]{1,0:T(8,128)(2,1)} %param.42, bf16[256,1024]{1,0:T(8,128)(2,1)S(1)} %reshape.124, bf16[1024,32]{0,1:T(8,128)(2,1)} %param.41, f32[256,32]{0,1:T(8,128)S(1)} %fusion.46), kind=kOutput, calls=%fused_computation.1 | convolution fusion | flops 33865728 | bytes 1212416 | tf_op jit(solution)/shard_map/dot_general | solution.py:157
  62.4 1.0 reshape.125
  63.3 4.7 %all-to-all-start.2 = ((bf16[64,4,1024]{2,1,0:T(4,128)(2,1)}), bf16[64,4,1024]{2,1,0:T(4,128)(2,1)S(1)}, u32[]{:S(2)}, u32[]{:S(2)}) async-start(bf16[64,4,1024]{2,1,0:T(4,128)(2,1)} %reshape.125), calls=%async_computation.2 | async-start | bytes 1048576 | tf_op jit(solution)/shard_map/all_to_all | solution.py:41
  68.1 1.5 %fusion.12 = f32[128,352]{0,1:T(8,128)S(1)} fusion(bf16[128,1024]{1,0:T(8,128)(2,1)S(1)} %all_to_all.25, bf16[1,1024,352]{1,2,0:T(8,128)(2,1)} %param.37), kind=kOutput, calls=%fused_computation.23 | convolution fusion | flops 92274688 | bytes 1163264 | tf_op jit(solution)/shard_map/dot_general | solution.py:148
  69.6 2.2 %convolution_convert_fusion.1 = bf16[128,1024]{1,0:T(8,128)(2,1)S(1)} fusion(bf16[128,1024]{1,0:T(8,128)(2,1)S(1)} %all_to_all.25, bf16[1,352,1024]{2,1,0:T(8,128)(2,1)} %param.39, bf16[1,1024,352]{1,2,0:T(8,128)(2,1)} %param.38, f32[128,352]{0,1:T(8,128)S(1)} %fusion.12), kind=kOutput, calls=%fused_computation.2 | convolution fusion | flops 184950784 | bytes 2146304 | tf_op jit(solution)/shard_map/dot_general | solution.py:151
  71.8 8.3 %all-to-all-done.2 = bf16[64,4,1024]{2,1,0:T(4,128)(2,1)S(1)} async-done(((bf16[64,4,1024]{2,1,0:T(4,128)(2,1)}), bf16[64,4,1024]{2,1,0:T(4,128)(2,1)S(1)}, u32[]{:S(2)}, u32[]{:S(2)}) %all-to-all-start.2) | async-done | bytes 524320 | tf_op jit(solution)/shard_map/all_to_all | solution.py:41
  80.5 3.9 %all_to_all.37 = bf16[2,132,512]{2,1,0:T(8,128)(2,1)S(1)} all-to-all(bf16[2,132,512]{2,1,0:T(8,128)(2,1)S(1)} %bitcast.66), channel_id=1, replica_groups=mesh['ep'=64,'tp'=2] {'tp'}, dimensions={0} | all-to-all | bytes 540672 | tf_op jit(solution)/shard_map/all_to_all | solution.py:41
  84.5 0.7 all_to_all.29
  85.2 4.7 %all-to-all-start.4 = ((bf16[64,2,512]{2,1,0:T(2,128)(2,1)}), bf16[64,2,512]{2,1,0:T(2,128)(2,1)S(1)}, u32[]{:S(2)}, u32[]{:S(2)}) async-start(bf16[64,2,512]{2,1,0:T(2,128)(2,1)} %all_to_all.29), calls=%async_computation.4 | async-start | bytes 262144 | tf_op jit(solution)/shard_map/all_to_all | solution.py:164
  90.1 9.8 %all-to-all-done.4 = bf16[64,2,512]{2,1,0:T(2,128)(2,1)S(1)} async-done(((bf16[64,2,512]{2,1,0:T(2,128)(2,1)}), bf16[64,2,512]{2,1,0:T(2,128)(2,1)S(1)}, u32[]{:S(2)}, u32[]{:S(2)}) %all-to-all-start.4) | async-done | bytes 131104 | tf_op jit(solution)/shard_map/all_to_all | solution.py:164
  100.0 0.8 fusion.7
  (75 shorter events, 4.4 us)
Async XLA Ops:
  0.6 1.8 %copy-start = (bf16[1024,1024]{1,0:T(8,128)(2,1)S(1)}, bf16[1024,1024]{1,0:T(8,128)(2,1)}, u32[]{:S(2)}) copy-start(bf16[1024,1024]{1,0:T(8,128)(2,1)} %param.24) | copy-start | bytes 6291460
  0.6 2.2 %copy-start.7 = (s32[4,2]{0,1:T(2,128)S(1)}, s32[4,2]{0,1:T(2,128)}, u32[]{:S(2)}) copy-start(s32[4,2]{0,1:T(2,128)} %param.35) | copy-start | bytes 100
  0.7 2.4 %copy-start.11 = (bf16[1024,2]{0,1:T(2,128)(2,1)S(1)}, bf16[1024,2]{0,1:T(2,128)(2,1)}, u32[]{:S(2)}) copy-start(bf16[1024,2]{0,1:T(2,128)(2,1)} %param.27) | copy-start | bytes 12292
  0.7 2.5 %copy-start.13 = (f32[4,2]{0,1:T(2,128)S(1)}, f32[4,2]{0,1:T(2,128)}, u32[]{:S(2)}) copy-start(f32[4,2]{0,1:T(2,128)} %param.33) | copy-start | bytes 100
  0.7 2.5 %copy-start.14 = (f32[2]{0:T(128)S(1)}, f32[2]{0:T(128)}, u32[]{:S(2)}) copy-start(f32[2]{0:T(128)} %param.29) | copy-start | bytes 28
  0.7 2.5 %copy-start.12 = (bf16[1024,2]{0,1:T(2,128)(2,1)S(1)}, bf16[1024,2]{0,1:T(2,128)(2,1)}, u32[]{:S(2)}) copy-start(bf16[1024,2]{0,1:T(2,128)(2,1)} %param.28) | copy-start | bytes 12292
  2.5 3.1 %copy-start.5 = (f32[4,2,512]{2,1,0:T(2,128)S(1)}, f32[4,2,512]{2,1,0:T(2,128)}, u32[]{:S(2)}) copy-start(f32[4,2,512]{2,1,0:T(2,128)} %param.32) | copy-start | bytes 49156
  3.3 5.1 %copy-start.8 = (f32[4,2]{0,1:T(2,128)}, f32[4,2]{0,1:T(2,128)S(1)}, u32[]{:S(2)}) copy-start(f32[4,2]{0,1:T(2,128)S(1)} %get-tuple-element.10) | copy-start | bytes 100
  12.5 3.5 %copy-start.1 = (f32[4,2,512,512]{3,2,1,0:T(8,128)}, f32[4,2,512,512]{3,2,1,0:T(8,128)S(1)}, u32[]{:S(2)}) copy-start(f32[4,2,512,512]{3,2,1,0:T(8,128)S(1)} %multiply_add_fusion) | copy-start | bytes 25165828
  12.5 3.6 %copy-start.2 = (bf16[1024,1024]{1,0:T(8,128)(2,1)S(1)}, bf16[1024,1024]{1,0:T(8,128)(2,1)}, u32[]{:S(2)}) copy-start(bf16[1024,1024]{1,0:T(8,128)(2,1)} %param.30) | copy-start | bytes 6291460
  16.1 2.3 %copy-start.3 = (bf16[4,1024]{1,0:T(4,128)(2,1)S(1)}, bf16[4,1024]{1,0:T(4,128)(2,1)}, u32[]{:S(2)}) copy-start(bf16[4,1024]{1,0:T(4,128)(2,1)} %param.22) | copy-start | bytes 24580
  16.1 3.1 %copy-start.6 = (f32[1024]{0:T(1024)S(1)}, f32[1024]{0:T(1024)}, u32[]{:S(2)}) copy-start(f32[1024]{0:T(1024)} %param.34) | copy-start | bytes 12292
  16.2 31.5 %copy-start.10 = (f32[4,2]{0,1:T(2,128)S(1)}, f32[4,2]{0,1:T(2,128)}, u32[]{:S(2)}) copy-start(f32[4,2]{0,1:T(2,128)} %param.36) | copy-start | bytes 100
  18.5 41.9 %copy-start.4 = (bf16[1024,32]{0,1:T(8,128)(2,1)S(1)}, bf16[1024,32]{0,1:T(8,128)(2,1)}, u32[]{:S(2)}) copy-start(bf16[1024,32]{0,1:T(8,128)(2,1)} %param.40) | copy-start | bytes 196612
  42.8 17.4 %all-to-all-start.1 = ((bf16[64,4,1024]{2,1,0:T(4,128)(2,1)}), bf16[64,4,1024]{2,1,0:T(4,128)(2,1)S(1)}, u32[]{:S(2)}, u32[]{:S(2)}) async-start(bf16[64,4,1024]{2,1,0:T(4,128)(2,1)} %broadcast_in_dim.5), calls=%async_computation.1 | async-start | bytes 1048576 | tf_op jit(solution)/shard_map/all_to_all | solution.py:19
  63.3 16.7 %all-to-all-start.2 = ((bf16[64,4,1024]{2,1,0:T(4,128)(2,1)}), bf16[64,4,1024]{2,1,0:T(4,128)(2,1)S(1)}, u32[]{:S(2)}, u32[]{:S(2)}) async-start(bf16[64,4,1024]{2,1,0:T(4,128)(2,1)} %reshape.125), calls=%async_computation.2 | async-start | bytes 1048576 | tf_op jit(solution)/shard_map/all_to_all | solution.py:41
  71.8 28.2 %copy-start.9 = (f32[512]{0:T(512)S(1)}, f32[512]{0:T(512)}, u32[]{:S(2)}) copy-start(f32[512]{0:T(512)} %param.43) | copy-start | bytes 6148
  85.2 14.7 %all-to-all-start.4 = ((bf16[64,2,512]{2,1,0:T(2,128)(2,1)}), bf16[64,2,512]{2,1,0:T(2,128)(2,1)S(1)}, u32[]{:S(2)}, u32[]{:S(2)}) async-start(bf16[64,2,512]{2,1,0:T(2,128)(2,1)} %all_to_all.29), calls=%async_computation.4 | async-start | bytes 262144 | tf_op jit(solution)/shard_map/all_to_all | solution.py:164
where the time goes:
time: 101 us
  waiting for transfers between devices  30.4 us (30%)
  blocking collectives  28 us (28%)
  matrix products  14.7 us (15%)
  starting transfers between devices  14.3 us (14%)
  other arithmetic  7.66 us (8%)
  local copies, waits for them, and re-layouts  4.79 us (5%)
    all_to_all x1, blocking collectives, shards(): lax.all_to_all(outgoing, 'ep', split_axis=0, concat_axis=0, tiled=True)  22.3 us
    all_to_all x1, waiting for transfers between devices, copy_for_each(): return lax.all_to_all(copies, axis, split_axis=0, concat_axis=0, tiled=True)  12.3 us
    all_to_all x1, waiting for transfers between devices, shards(): lax.all_to_all(expert_half.astype(jnp.bfloat16), 'ep', split_axis=0, conc...  9.77 us
    all_to_all x1, waiting for transfers between devices, sent_and_summed(): lax.all_to_all(blocks, axis, split_axis=0, concat_axis=0, tiled=True)  8.28 us
    all_to_all x1, starting transfers between devices, copy_for_each(): return lax.all_to_all(copies, axis, split_axis=0, concat_axis=0, tiled=True)  4.86 us
    all_to_all x1, starting transfers between devices, sent_and_summed(): lax.all_to_all(blocks, axis, split_axis=0, concat_axis=0, tiled=True)  4.73 us
    all_to_all x1, starting transfers between devices, shards(): lax.all_to_all(expert_half.astype(jnp.bfloat16), 'ep', split_axis=0, conc...  4.73 us
    add x1, other arithmetic, cell_step(): carry[..., None, None] * memory  4.04 us
  transfers between devices with their start and end apart: 3, of which 3 were waited for; matrix products, arithmetic and copies ran while one was open for 4% of the time, Pallas kernels for 0%

commit v1 on v0

v1 whole, which is shorter than its diff:
```python
import functools

import jax
import jax.numpy as jnp
from jax import lax
from jax.experimental import pallas as pl
from jax.experimental.pallas import tpu as pltpu
from jax.sharding import PartitionSpec as P

EXPERTS = 8
RING = 4
PLANE = 16
ROWS = 4
BLOCK = 16
TOKENS = 256
WIDTH = 1024
HALF = 512
UNITS = 352
DENSE = 32
ALL_UNITS = 384
MESH = pl.DeviceIdType.MESH
F32 = jnp.float32
BF16 = jnp.bfloat16
EPSILON = 1e-06
OFFSETS = sorted(
    [(dz, dy) for dz in range(RING) for dy in range(RING) if (dz, dy) != (0, 0)],
    key=lambda o: -(min(o[0], RING - o[0]) + min(o[1], RING - o[1])),
)


def normalize(values_in, gain):
    values = values_in.astype(F32)
    scale = lax.rsqrt(jnp.mean(values * values, axis=-1, keepdims=True) + EPSILON)
    return (values * scale * gain).astype(BF16)


def ffn_kernel(
    tokens_ref,
    partial_ref,
    gain_ref,
    ids_ref,
    weights_ref,
    scale_ref,
    gate_hbm,
    up_hbm,
    down_hbm,
    dense_gate_hbm,
    dense_up_hbm,
    dense_down_hbm,
    out_ref,
    other_partial,
    scales,
    stream,
    own_rows,
    row_in,
    weight_row,
    weight_in,
    gathered,
    weight_table,
    w_in,
    w_down,
    part_out,
    part_in,
    part_own,
    block_out,
    block_in,
    piece_out,
    piece_in,
    load_sem,
    pair_send,
    pair_recv,
    row_send,
    row_recv,
    plane_send,
    plane_recv,
    share_send,
    share_recv,
    sum_send,
    sum_recv,
    back_send,
    back_recv,
    piece_send,
    piece_recv,
):
    chip = lax.axis_index("ep")
    core = lax.axis_index("tp")
    other = 1 - core
    place = chip // RING
    x = lax.rem(chip, RING)
    z, y = place // RING, lax.rem(place, RING)

    def to(chip_at, core_at):
        return {"ep": chip_at, "tp": core_at}

    def plane_at(dz, dy):
        return lax.rem(z + dz, RING) * RING + lax.rem(y + dy, RING)

    def send(src, dst, send_sem, recv_sem, chip_at, core_at):
        copy = pltpu.make_async_remote_copy(
            src_ref=src,
            dst_ref=dst,
            send_sem=send_sem,
            recv_sem=recv_sem,
            device_id=to(chip_at, core_at),
            device_id_type=MESH,
        )
        copy.start()
        return copy

    barrier = pltpu.get_barrier_semaphore()
    pl.semaphore_signal(barrier, inc=1, device_id=to(chip, other), device_id_type=MESH)
    for d in range(1, RING):
        pl.semaphore_signal(
            barrier,
            inc=1,
            device_id=to(place * RING + lax.rem(x + d, RING), core),
            device_id_type=MESH,
        )
    for dz, dy in OFFSETS:
        pl.semaphore_signal(
            barrier,
            inc=1,
            device_id=to(plane_at(dz, dy) * RING + x, core),
            device_id_type=MESH,
        )

    loads = [
        (gate_hbm, w_in.at[pl.ds(0, UNITS)]),
        (dense_gate_hbm, w_in.at[pl.ds(UNITS, DENSE)]),
        (up_hbm, w_in.at[pl.ds(ALL_UNITS, UNITS)]),
        (dense_up_hbm, w_in.at[pl.ds(ALL_UNITS + UNITS, DENSE)]),
        (down_hbm.at[:, pl.ds(0, HALF)], w_down.at[0, pl.ds(0, UNITS)]),
        (down_hbm.at[:, pl.ds(HALF, HALF)], w_down.at[1, pl.ds(0, UNITS)]),
        (dense_down_hbm.at[:, pl.ds(0, HALF)], w_down.at[0, pl.ds(UNITS, DENSE)]),
        (dense_down_hbm.at[:, pl.ds(HALF, HALF)], w_down.at[1, pl.ds(UNITS, DENSE)]),
    ]
    loading = []
    for i, (src, dst) in enumerate(loads):
        copy = pltpu.make_async_copy(src, dst, load_sem.at[i])
        copy.start()
        loading.append(copy)

    pl.semaphore_wait(barrier, 1 + RING - 1 + PLANE - 1)

    pending = []
    pair = [
        send(partial_ref, other_partial, pair_send.at[0], pair_recv.at[0], chip, other),
        send(scale_ref, scales.at[core], pair_send.at[1], pair_recv.at[1], chip, other),
    ]
    scales[core] = scale_ref[...]
    lane = lax.broadcasted_iota(jnp.int32, (1, 128), 1)
    row = jnp.zeros((1, 128), F32)
    for i in range(ROWS):
        for k in range(2):
            hit = lane == x * (ROWS * EXPERTS) + i * EXPERTS + ids_ref[k, i]
            row = row + jnp.where(hit, weights_ref[k, i], 0.0)
    weight_row[...] = row
    for d in range(1, RING):
        q = place * RING + lax.rem(x + d, RING)
        pending.append(
            send(weight_row, weight_in.at[d], row_send.at[1, d], row_recv.at[1, d], q, core)
        )
    pair[0].wait_recv()
    mixed = partial_ref[...].astype(F32) + other_partial[...].astype(F32)
    total = tokens_ref[...].astype(F32) + mixed
    stream[0] = total[:, :HALF]
    stream[1] = total[:, HALF:]
    ffn_in = normalize(total, gain_ref[...])
    own_rows[0] = ffn_in[:, :HALF]
    own_rows[1] = ffn_in[:, HALF:]
    for d in range(1, RING):
        q = place * RING + lax.rem(x + d, RING)
        pending.append(
            send(own_rows.at[core], row_in.at[x], row_send.at[0, d], row_recv.at[0, d], q, core)
        )
    row_in[x] = own_rows[core]
    for d in range(1, RING):
        pending[d - 1].wait_recv()
        row = row + weight_in[d]
    weight_table[pl.ds(place, 1), :] = row
    for d in range(1, RING):
        pending[RING - 1 + d - 1].wait_recv()
    rows16 = jnp.concatenate([row_in[j].astype(F32) for j in range(RING)], axis=0)
    own_block = gathered.at[core, pl.ds(pl.multiple_of(place * BLOCK, BLOCK), BLOCK)]
    own_block[...] = rows16.astype(BF16)

    arriving = []
    for i, (dz, dy) in enumerate(OFFSETS):
        q = plane_at(dz, dy) * RING + x
        arriving.append(
            (
                send(own_block, own_block, plane_send.at[0, i], plane_recv.at[0, i], q, core),
                send(
                    weight_table.at[pl.ds(place, 1)],
                    weight_table.at[pl.ds(place, 1)],
                    plane_send.at[1, i],
                    plane_recv.at[1, i],
                    q,
                    core,
                ),
            )
        )
    shared = [send(own_block, own_block, share_send.at[PLANE - 1], share_recv.at[PLANE - 1], chip, other)]
    for i in reversed(range(PLANE - 1)):
        dz, dy = OFFSETS[i]
        arriving[i][0].wait_recv()
        came = plane_at(RING - dz, RING - dy)
        block = gathered.at[core, pl.ds(pl.multiple_of(came * BLOCK, BLOCK), BLOCK)]
        shared.append(send(block, block, share_send.at[i], share_recv.at[i], chip, other))

    for copy in loading:
        copy.wait()
    pair[1].wait_recv()
    for half in range(2):
        w_down[half, UNITS:, :] = (
            w_down[half, UNITS:, :].astype(F32) * scales[half]
        ).astype(BF16)
    for i in range(PLANE - 1):
        arriving[i][1].wait_recv()
    expert = chip // EXPERTS
    sub = lax.broadcasted_iota(jnp.int32, (BLOCK, 128), 0)
    lane16 = lax.broadcasted_iota(jnp.int32, (BLOCK, 128), 1)
    picked = lane16 == sub * EXPERTS + expert
    table = weight_table[...]
    columns = [
        jnp.sum(jnp.where(picked, table[g : g + 1, :], 0.0), axis=1, keepdims=True)
        for g in range(PLANE)
    ]
    column = jnp.concatenate(columns, axis=0)

    for copy in shared:
        copy.wait_recv()
    nt = (((1,), (1,)), ((), ()))
    raised = lax.dot_general(
        gathered[0], w_in[:, :HALF], nt, preferred_element_type=F32
    ) + lax.dot_general(gathered[1], w_in[:, HALF:], nt, preferred_element_type=F32)
    gated = raised[:, :ALL_UNITS]
    lifted = raised[:, ALL_UNITS:]
    unit = lax.broadcasted_iota(jnp.int32, (TOKENS, ALL_UNITS), 1)
    hidden = gated / (1.0 + jnp.exp(-gated)) * lifted * jnp.where(unit < UNITS, column, 1.0)
    hidden = hidden.astype(BF16)
    part_out[...] = jnp.dot(hidden, w_down[other], preferred_element_type=F32).astype(BF16)
    swap = send(part_out, part_in, sum_send.at[0], sum_recv.at[0], chip, other)
    part_own[...] = jnp.dot(hidden, w_down[core], preferred_element_type=F32)
    swap.wait_recv()
    summed = part_own[...] + part_in[...].astype(F32)
    block_out[...] = summed.astype(BF16)
    part_own[...] = summed
    back = []
    for i, (dz, dy) in enumerate(OFFSETS):
        q = plane_at(dz, dy)
        block = block_out.at[pl.ds(pl.multiple_of(q * BLOCK, BLOCK), BLOCK)]
        back.append(
            send(block, block_in.at[i], back_send.at[i], back_recv.at[i], q * RING + x, core)
        )
    total = part_own[pl.ds(pl.multiple_of(place * BLOCK, BLOCK), BLOCK), :]
    for i in reversed(range(PLANE - 1)):
        back[i].wait_recv()
        total = total + block_in[i].astype(F32)
    for j in range(RING):
        piece_out[j] = total[j * ROWS : (j + 1) * ROWS, :].astype(BF16)
    pieces = []
    for d in range(1, RING):
        at = lax.rem(x + d, RING)
        pieces.append(
            send(
                piece_out.at[at],
                piece_in.at[d],
                piece_send.at[d],
                piece_recv.at[d],
                place * RING + at,
                core,
            )
        )
    result = stream[core] + piece_out[x].astype(F32)
    for copy in pieces:
        copy.wait_recv()
    for d in range(1, RING):
        result = result + piece_in[d].astype(F32)
    out_ref[...] = result.astype(BF16)

    for copy in pair + pending + shared + [swap] + back + pieces:
        copy.wait_send()
    for a, b in arriving:
        a.wait_send()
        b.wait_send()


def ffn(tokens, partial, ffn_gain, ids, weights, scale, gate, up, down, dense_gate, dense_up, dense_down):
    vmem = pl.BlockSpec(memory_space=pltpu.VMEM)
    smem = pl.BlockSpec(memory_space=pltpu.SMEM)
    hbm = pl.BlockSpec(memory_space=pl.ANY)
    dma = pltpu.SemaphoreType.DMA
    return pl.pallas_call(
        ffn_kernel,
        out_shape=jax.ShapeDtypeStruct((ROWS, HALF), BF16),
        in_specs=[vmem, vmem, vmem, smem, smem, vmem] + [hbm] * 6,
        out_specs=vmem,
        scratch_shapes=[
            pltpu.VMEM((ROWS, WIDTH), BF16),
            pltpu.VMEM((2, 1, HALF), F32),
            pltpu.VMEM((2, ROWS, HALF), F32),
            pltpu.VMEM((2, ROWS, HALF), BF16),
            pltpu.VMEM((RING, ROWS, HALF), BF16),
            pltpu.VMEM((1, 128), F32),
            pltpu.VMEM((RING, 1, 128), F32),
            pltpu.VMEM((2, TOKENS, HALF), BF16),
            pltpu.VMEM((PLANE, 128), F32),
            pltpu.VMEM((2 * ALL_UNITS, WIDTH), BF16),
            pltpu.VMEM((2, ALL_UNITS, HALF), BF16),
            pltpu.VMEM((TOKENS, HALF), BF16),
            pltpu.VMEM((TOKENS, HALF), BF16),
            pltpu.VMEM((TOKENS, HALF), F32),
            pltpu.VMEM((TOKENS, HALF), BF16),
            pltpu.VMEM((PLANE, BLOCK, HALF), BF16),
            pltpu.VMEM((RING, ROWS, HALF), BF16),
            pltpu.VMEM((RING, ROWS, HALF), BF16),
            dma((8,)),
            dma((2,)),
            dma((2,)),
            dma((2, RING)),
            dma((2, RING)),
            dma((2, PLANE)),
            dma((2, PLANE)),
            dma((PLANE,)),
            dma((PLANE,)),
            dma((1,)),
            dma((1,)),
            dma((PLANE,)),
            dma((PLANE,)),
            dma((RING,)),
            dma((RING,)),
        ],
        compiler_params=pltpu.CompilerParams(
            collective_id=0, has_side_effects=True, vmem_limit_bytes=32 * 2**20
        ),
    )(tokens, partial, ffn_gain, ids, weights, scale, gate, up, down, dense_gate, dense_up, dense_down)


def cell_step(
    query_heads, key_heads, value_heads, in_gate, forget_log, memory, normalizer, stabilizer
):
    new_stabilizer = jnp.maximum(forget_log + stabilizer, in_gate)
    carry = jnp.exp(forget_log + stabilizer - new_stabilizer)
    admit = jnp.exp(in_gate - new_stabilizer)
    scaled_key = admit[..., None] * key_heads
    new_memory = (
        carry[..., None, None] * memory + scaled_key[..., :, None] * value_heads[..., None, :]
    )
    new_normalizer = carry[..., None] * normalizer + scaled_key
    numer = jnp.einsum(
        "...hd,...hde->...he", query_heads, new_memory, precision=lax.Precision.HIGHEST
    )
    denom = jnp.sum(new_normalizer * query_heads, axis=-1)
    bound = jnp.maximum(jnp.abs(denom), jnp.exp(-new_stabilizer))
    return (numer / bound[..., None], new_memory, new_normalizer, new_stabilizer)


def shards(
    tokens,
    mixer_gain,
    w_query,
    w_key,
    w_value,
    w_input_gate,
    w_forget_gate,
    forget_bias,
    w_output,
    memory,
    normalizer,
    stabilizer,
    ffn_gain,
    route_ids,
    route_weights,
    expert_gate,
    expert_up,
    expert_down,
    dense_gate_w,
    dense_up_w,
    dense_down_w,
    dense_scale,
):
    local_rows = tokens.shape[0]
    local_heads = memory.shape[1]
    head_size = memory.shape[2]
    width = tokens.shape[1]
    normed = normalize(tokens, mixer_gain)
    query = jnp.dot(normed, w_query, preferred_element_type=jnp.float32).astype(jnp.bfloat16)
    key = jnp.dot(normed, w_key, preferred_element_type=jnp.float32).astype(jnp.bfloat16)
    value = jnp.dot(normed, w_value, preferred_element_type=jnp.float32).astype(jnp.bfloat16)
    in_gate = jnp.dot(normed, w_input_gate, preferred_element_type=jnp.float32)
    forget_log = jax.nn.log_sigmoid(
        jnp.dot(normed, w_forget_gate, preferred_element_type=jnp.float32) + forget_bias
    )
    shaped = (local_rows, local_heads, head_size)
    query_heads = query.astype(jnp.float32).reshape(shaped)
    key_heads = key.astype(jnp.float32).reshape(shaped) * head_size ** (-0.5)
    value_heads = value.astype(jnp.float32).reshape(shaped)
    read, new_memory, new_normalizer, new_stabilizer = cell_step(
        query_heads, key_heads, value_heads, in_gate, forget_log, memory, normalizer, stabilizer
    )
    read = read.reshape(local_rows, local_heads * head_size).astype(jnp.bfloat16)
    partial_value = jnp.dot(read, w_output, preferred_element_type=jnp.float32)
    output = ffn(
        tokens,
        partial_value.astype(jnp.bfloat16),
        ffn_gain.reshape(1, width),
        route_ids.T,
        route_weights.T,
        dense_scale.reshape(1, -1),
        expert_gate[0].T,
        expert_up[0].T,
        expert_down[0],
        dense_gate_w.T,
        dense_up_w.T,
        dense_down_w,
    )
    return (output, new_memory, new_normalizer, new_stabilizer)


def solution(mesh):
    placed = (
        P("ep", None),
        P(),
        P(None, "tp"),
        P(None, "tp"),
        P(None, "tp"),
        P(None, "tp"),
        P(None, "tp"),
        P("tp"),
        P("tp", None),
        P("ep", "tp", None, None),
        P("ep", "tp", None),
        P("ep", "tp"),
        P(),
        P("ep", None),
        P("ep", None),
        P("ep", None, "tp"),
        P("ep", None, "tp"),
        P("ep", "tp", None),
        P(None, ("ep", "tp")),
        P(None, ("ep", "tp")),
        P(("ep", "tp"), None),
        P("tp"),
    )
    return jax.shard_map(
        shards,
        mesh=mesh,
        in_specs=placed,
        out_specs=(P("ep", "tp"), P("ep", "tp", None, None), P("ep", "tp", None), P("ep", "tp")),
        check_vma=False,
    )
```

time: 101 us -> 67.3 us (0.67)
  Pallas kernels: 0 us -> 31.8 us
  waiting for transfers between devices: 30.4 us -> 0 us
  blocking collectives: 28 us -> 0 us
  starting transfers between devices: 14.3 us -> 0 us
  other arithmetic: 7.66 us -> 11.3 us
  local copies, waits for them, and re-layouts: 4.79 us -> 8.11 us
    pallas_call x0 -> x1, Pallas kernels: none -> 31.8 us  [ffn(): pl.pallas_call(ffn_kernel, out_shape=jax.ShapeDtypeStruct((ROWS, HALF), B...]
    all_to_all x3 -> x0, waiting for transfers between devices: 30.4 us -> none  [the longest x1 12.3 us: copy_for_each(): return lax.all_to_all(copies, axis, split_axis=0, concat_axis=0, tiled=True)]
    all_to_all x2 -> x0, blocking collectives: 26.2 us -> none  [the longest x1 22.3 us: shards(): lax.all_to_all(outgoing, 'ep', split_axis=0, concat_axis=0, tiled=True)]
    all_to_all x3 -> x0, starting transfers between devices: 14.3 us -> none  [the longest x1 4.86 us: copy_for_each(): return lax.all_to_all(copies, axis, split_axis=0, concat_axis=0, tiled=True)]
    dot_general x7 -> x0, matrix products: 6.81 us -> none  [the longest x1 2.2 us: shards(): jnp.dot(expert_hidden, expert_down[0], preferred_element_type=jnp.float32)]
    unnamed x33 -> x30, local copies, waits for them, and re-layouts: 0.88 us -> 5.07 us
    dot_general x1, matrix products: 2.91 us -> 6.73 us  [cell_step(): jnp.einsum('...hd,...hde->...he', query_heads, new_memory, precision=lax....]
    add x1, other arithmetic: 4.04 us -> 6.12 us  [cell_step(): carry[..., None, None] * memory]
  transfers between devices with their start and end apart: 3 -> 0, of which waited for: 3 -> 0; matrix products, arithmetic and copies ran while one was open for 4% -> 0% of each run, Pallas kernels for 0% -> 0%
where the time goes in v1:
time: 67.3 us; the launch traced here: 66.7 us
  Pallas kernels  31.8 us (47%)
  matrix products  14.7 us (22%)
  other arithmetic  11.3 us (17%)
  local copies, waits for them, and re-layouts  8.11 us (12%)
  between operations  0.76 us (1%)
    pallas_call x1, Pallas kernels, ffn(): pl.pallas_call(ffn_kernel, out_shape=jax.ShapeDtypeStruct((ROWS, HALF), B...  31.8 us
    dot_general x1, matrix products, cell_step(): jnp.einsum('...hd,...hde->...he', query_heads, new_memory, precision=lax....  6.73 us
    add x1, other arithmetic, cell_step(): carry[..., None, None] * memory  6.12 us
    unnamed x30, local copies, waits for them, and re-layouts  5.07 us
    dot_general x1, matrix products, shards(): jnp.dot(normed, w_key, preferred_element_type=jnp.float32)  1.98 us
    dot_general x1, matrix products, shards(): partial_value = jnp.dot(read, w_output, preferred_element_type=jnp.float32)  1.98 us
    dot_general x1, matrix products, shards(): jnp.dot(normed, w_value, preferred_element_type=jnp.float32)  1.97 us
    reduce_sum x1, local copies, waits for them, and re-layouts, cell_step(): denom = jnp.sum(new_normalizer * query_heads, axis=-1)  1.44 us

profile of v1, /device:TPU:0, one launch (start us, length us, event | category | flops | bytes accessed | tf_op | source)
XLA Modules:
  0.0 66.7 jit_solution(6419629532015517796)
XLA Ops:
  0.6 1.0 %fusion.3 = f32[4]{0:T(128)S(1)} fusion(bf16[4,1024]{1,0:T(4,128)(2,1)} %tokens_ref.1), kind=kLoop, calls=%fused_computation.11 | loop fusion | flops 12284 | bytes 8208 | tf_op jit(solution)/shard_map/reduce_sum | solution.py:33
  1.6 0.8 %fusion.5 = bf16[4,1024]{1,0:T(4,128)(2,1)S(1)} fusion(bf16[4,1024]{1,0:T(4,128)(2,1)} %tokens_ref.1, f32[1024]{0:T(1024)} %param.23, f32[4]{0:T(128)S(1)} %add_rsqrt_fusion), kind=kLoop, calls=%fused_computation.13 | loop fusion | flops 16384 | bytes 20496 | tf_op jit(solution)/shard_map/convert_element_type | solution.py:34
  2.4 0.8 %fusion.10 = f32[4,2]{0,1:T(2,128)S(1)} fusion(bf16[4,1024]{1,0:T(4,128)(2,1)S(1)} %fusion.5, bf16[1024,2]{0,1:T(2,128)(2,1)} %param.27), kind=kOutput, calls=%fused_computation.27 | convolution fusion | flops 16384 | bytes 12320 | tf_op jit(solution)/shard_map/dot_general | solution.py:391
  3.2 0.8 %subtract_exponential_fusion = (f32[4,2]{0,1:T(2,128)S(1)}, f32[4,2]{0,1:T(2,128)S(1)}) fusion(f32[4,2]{0,1:T(2,128)S(1)} %fusion.10, f32[4,2]{0,1:T(2,128)} %param.33, f32[2]{0:T(128)} %param.29, bf16[4,1024]{1,0:T(4,128)(2,1)S(1)} %fusion.5, bf16[1024,2]{0,1:T(2,128)(2,1)} %param.28), kind=kOutput, calls=%fused_computation.25 | convolution fusion | flops 16480 | bytes 12424 | tf_op jit(solution)/shard_map/dot_general | solution.py:393
  4.1 0.6 copy-done.13
  4.6 0.1 copy.31
  4.8 0.4 convolution_convert_fusion.3
  5.2 2.0 %fusion.1 = f32[4,1024]{1,0:T(4,128)S(1)} fusion(bf16[4,1024]{1,0:T(4,128)(2,1)S(1)} %fusion.5, bf16[1024,1024]{1,0:T(8,128)(2,1)} %param.25), kind=kOutput, calls=%fused_computation.5 | convolution fusion | flops 8396800 | bytes 2121728 | tf_op jit(solution)/shard_map/dot_general | solution.py:389
  7.3 1.3 %multiply_reduce_fusion = (f32[4,2]{1,0:T(4,128)}, f32[4,2,512]{2,1,0:T(2,128)}, f32[4,2,512]{2,1,0:T(2,128)S(1)}) fusion(bf16[4,2,512]{2,1,0:T(2,128)(2,1)S(1)} %reshape.48, f32[4,2,512]{2,1,0:T(2,128)S(1)} %copy-done.12, f32[4,2]{1,0:T(4,128)S(1)} %copy.30, f32[4,2,512]{2,1,0:T(2,128)S(1)} %reshape.55, f32[4,2]{1,0:T(4,128)S(1)} %copy.31), kind=kLoop, calls=%fused_computation.15 | loop fusion | flops 24568 | bytes 73824 | tf_op jit(solution)/shard_map/reduce_sum | solution.py:354
  8.5 2.0 %fusion = f32[4,1024]{1,0:T(4,128)S(1)} fusion(bf16[4,1024]{1,0:T(4,128)(2,1)S(1)} %fusion.5, bf16[1024,1024]{1,0:T(8,128)(2,1)} %param.26), kind=kOutput, calls=%fused_computation.3 | convolution fusion | flops 8396800 | bytes 2121728 | tf_op jit(solution)/shard_map/dot_general | solution.py:390
  10.5 6.1 %multiply_add_fusion = f32[4,2,512,512]{3,2,1,0:T(8,128)} fusion(f32[4,2,512,512]{3,2,1,0:T(8,128)} %param.31, f32[4,2,512]{2,1,0:T(2,128)S(1)} %reshape.56, f32[4,2,512]{2,1,0:T(2,128)S(1)} %get-tuple-element.6, f32[4,2]{1,0:T(4,128)S(1)} %copy.30), kind=kLoop, calls=%fused_computation | loop fusion | flops 6291456 | bytes 16810016 | tf_op jit(solution)/shard_map/add | solution.py:348
  16.7 6.7 %fusion.11 = f32[4,2,1,512]{3,2,1,0:T(1,128)} fusion(bf16[4,2,512,1]{2,3,1,0:T(2,128)(2,1)S(1)} %reshape.60, f32[4,2,512,512]{3,2,1,0:T(8,128)} %multiply_add_fusion), kind=kOutput, calls=%fused_computation.28 | convolution fusion | flops 25165824 | bytes 8413184 | tf_op jit(solution)/shard_map/...hd,...hde->...he/dot_general | solution.py:351
  23.4 1.4 %copy.33 = f32[4,2]{0,1:T(2,128)} copy(f32[4,2]{1,0:T(4,128)} %get-tuple-element.4) | data formatting | bytes 64 | tf_op jit(solution)/shard_map/reduce_sum | solution.py:354
  24.9 1.3 %exponential_maximum_fusion = f32[4,2]{0,1:T(2,128)} fusion(f32[4,2]{0,1:T(2,128)} %copy-done.13, f32[4,2]{0,1:T(2,128)} %copy.33), kind=kLoop, calls=%fused_computation.23 | loop fusion | flops 24 | bytes 96 | tf_op jit(solution)/shard_map/max | solution.py:355
  26.1 1.3 %copy.34 = f32[4,2]{1,0:T(4,128)} copy(f32[4,2]{0,1:T(2,128)} %exponential_maximum_fusion) | data formatting | bytes 64 | tf_op jit(solution)/shard_map/max | solution.py:355
  27.5 0.9 %fusion.7 = bf16[1,4,2,512]{3,2,1,0:T(2,128)(2,1)S(1)} fusion(f32[4,2]{1,0:T(4,128)} %copy.34, f32[4,2,1,512]{3,2,1,0:T(1,128)} %fusion.11), kind=kLoop, calls=%fused_computation.19 | loop fusion | flops 8192 | bytes 24608
  28.4 2.0 %convolution_convert_fusion.partial_ref = bf16[4,1024]{1,0:T(4,128)(2,1)S(1)} fusion(bf16[4,1024]{1,0:T(4,128)(2,1)S(1)} %bitcast.45, bf16[1024,1024]{1,0:T(8,128)(2,1)} %param.30), kind=kOutput, calls=%fused_computation.1 | convolution fusion | flops 8392704 | bytes 2113536 | tf_op jit(solution)/shard_map/dot_general | solution.py:403
  30.4 0.8 %copy-done.5 = bf16[1024,32]{0,1:T(8,128)(2,1)S(1)} copy-done((bf16[1024,32]{0,1:T(8,128)(2,1)S(1)}, bf16[1024,32]{0,1:T(8,128)(2,1)}, u32[]{:S(2)}) %copy-start.5) | copy-done | bytes 65560
  31.2 0.8 %copy-done.6 = bf16[1024,32]{0,1:T(8,128)(2,1)S(1)} copy-done((bf16[1024,32]{0,1:T(8,128)(2,1)S(1)}, bf16[1024,32]{0,1:T(8,128)(2,1)}, u32[]{:S(2)}) %copy-start.6) | copy-done | bytes 65560
  32.1 0.8 %copy-done.7 = bf16[32,1024]{1,0:T(8,128)(2,1)S(1)} copy-done((bf16[32,1024]{1,0:T(8,128)(2,1)S(1)}, bf16[32,1024]{1,0:T(8,128)(2,1)}, u32[]{:S(2)}) %copy-start.7) | copy-done | bytes 65560
  32.9 0.7 %copy-done.10 = s32[4,2]{0,1:T(2,128)S(1)} copy-done((s32[4,2]{0,1:T(2,128)S(1)}, s32[4,2]{0,1:T(2,128)}, u32[]{:S(2)}) %copy-start.10) | copy-done | bytes 56
  33.6 0.7 %copy-done.11 = f32[4,2]{0,1:T(2,128)S(1)} copy-done((f32[4,2]{0,1:T(2,128)S(1)}, f32[4,2]{0,1:T(2,128)}, u32[]{:S(2)}) %copy-start.11) | copy-done | bytes 56
  34.3 31.8 %shard_map.237 = bf16[4,512]{1,0:T(4,128)(2,1)S(1)} custom-call(bf16[4,1024]{1,0:T(4,128)(2,1)S(1)} %copy-done.4, bf16[4,1024]{1,0:T(4,128)(2,1)S(1)} %convolution_convert_fusion.partial_ref, f32[1,1024]{1,0:T(1,128)S(1)} %bitcast.41, s32[2,4]{1,0:T(2,128)S(1)} %bitcast.43, f32[2,4]{1,0:T(2,128)S(1)} %bitcast.44, f32[1,512]{1,0:T(1,128)S(1)} %bitcast.42, ...), custom_call_target="tpu_custom_call" | custom-call | tf_op jit(solution)/shard_map/pallas_call | solution.py:294
  66.1 0.6 copy.44
  (30 shorter events, 0.2 us)
Async XLA Ops:
  0.6 4.2 %copy-start = (bf16[1024,1024]{1,0:T(8,128)(2,1)S(1)}, bf16[1024,1024]{1,0:T(8,128)(2,1)}, u32[]{:S(2)}) copy-start(bf16[1024,1024]{1,0:T(8,128)(2,1)} %param.24) | copy-start | bytes 6291460
  4.1 0.6 copy-start.13
  4.8 2.4 %copy-start.12 = (f32[4,2,512]{2,1,0:T(2,128)S(1)}, f32[4,2,512]{2,1,0:T(2,128)}, u32[]{:S(2)}) copy-start(f32[4,2,512]{2,1,0:T(2,128)} %param.32) | copy-start | bytes 49156
  23.4 6.9 %copy-start.1 = (bf16[1,1024,352]{1,2,0:T(8,128)(2,1)S(1)}, bf16[1,1024,352]{1,2,0:T(8,128)(2,1)}, u32[]{:S(2)}) copy-start(bf16[1,1024,352]{1,2,0:T(8,128)(2,1)} %param.37) | copy-start | bytes 2162692
  23.4 6.9 %copy-start.2 = (bf16[1,1024,352]{1,2,0:T(8,128)(2,1)S(1)}, bf16[1,1024,352]{1,2,0:T(8,128)(2,1)}, u32[]{:S(2)}) copy-start(bf16[1,1024,352]{1,2,0:T(8,128)(2,1)} %param.38) | copy-start | bytes 2162692
  23.4 6.9 %copy-start.4 = (bf16[4,1024]{1,0:T(4,128)(2,1)S(1)}, bf16[4,1024]{1,0:T(4,128)(2,1)}, u32[]{:S(2)}) copy-start(bf16[4,1024]{1,0:T(4,128)(2,1)} %tokens_ref.1) | copy-start | bytes 24580
  23.4 6.9 %copy-start.8 = (f32[1024]{0:T(1024)S(1)}, f32[1024]{0:T(1024)}, u32[]{:S(2)}) copy-start(f32[1024]{0:T(1024)} %param.34) | copy-start | bytes 12292
  23.4 6.9 %copy-start.9 = (f32[512]{0:T(512)S(1)}, f32[512]{0:T(512)}, u32[]{:S(2)}) copy-start(f32[512]{0:T(512)} %param.43) | copy-start | bytes 6148
  27.5 2.9 %copy-start.3 = (bf16[1,352,1024]{2,1,0:T(8,128)(2,1)S(1)}, bf16[1,352,1024]{2,1,0:T(8,128)(2,1)}, u32[]{:S(2)}) copy-start(bf16[1,352,1024]{2,1,0:T(8,128)(2,1)} %param.39) | copy-start | bytes 2162692
  30.4 0.8 %copy-start.5 = (bf16[1024,32]{0,1:T(8,128)(2,1)S(1)}, bf16[1024,32]{0,1:T(8,128)(2,1)}, u32[]{:S(2)}) copy-start(bf16[1024,32]{0,1:T(8,128)(2,1)} %param.40) | copy-start | bytes 196612
  31.2 0.8 %copy-start.6 = (bf16[1024,32]{0,1:T(8,128)(2,1)S(1)}, bf16[1024,32]{0,1:T(8,128)(2,1)}, u32[]{:S(2)}) copy-start(bf16[1024,32]{0,1:T(8,128)(2,1)} %param.41) | copy-start | bytes 196612
  32.1 0.8 %copy-start.7 = (bf16[32,1024]{1,0:T(8,128)(2,1)S(1)}, bf16[32,1024]{1,0:T(8,128)(2,1)}, u32[]{:S(2)}) copy-start(bf16[32,1024]{1,0:T(8,128)(2,1)} %dense_down_hbm.1) | copy-start | bytes 196612
  32.9 0.7 %copy-start.10 = (s32[4,2]{0,1:T(2,128)S(1)}, s32[4,2]{0,1:T(2,128)}, u32[]{:S(2)}) copy-start(s32[4,2]{0,1:T(2,128)} %param.35) | copy-start | bytes 100
  33.6 0.7 %copy-start.11 = (f32[4,2]{0,1:T(2,128)S(1)}, f32[4,2]{0,1:T(2,128)}, u32[]{:S(2)}) copy-start(f32[4,2]{0,1:T(2,128)} %param.36) | copy-start | bytes 100

commit v2 on v1

--- a/solution.py
+++ b/solution.py
@@ -15,9 +15,15 @@
 TOKENS = 256
 WIDTH = 1024
 HALF = 512
+K2_VMEM = 40 * 2**20
+K1_VMEM = 40 * 2**20
 UNITS = 352
 DENSE = 32
 ALL_UNITS = 384
+HEADS = 2
+HEAD_SIZE = 512
+PAIRS = 8
+CHUNK = 64
 MESH = pl.DeviceIdType.MESH
 F32 = jnp.float32
 BF16 = jnp.bfloat16
@@ -36,11 +42,12 @@
 
 def ffn_kernel(
     tokens_ref,
-    partial_ref,
+    read_ref,
     gain_ref,
     ids_ref,
     weights_ref,
     scale_ref,
+    output_hbm,
     gate_hbm,
     up_hbm,
     down_hbm,
@@ -48,6 +55,8 @@
     dense_up_hbm,
     dense_down_hbm,
     out_ref,
+    w_output,
+    partial_ref,
     other_partial,
     scales,
     stream,
@@ -125,6 +134,7 @@
         )
 
     loads = [
+        (output_hbm, w_output),
         (gate_hbm, w_in.at[pl.ds(0, UNITS)]),
         (dense_gate_hbm, w_in.at[pl.ds(UNITS, DENSE)]),
         (up_hbm, w_in.at[pl.ds(ALL_UNITS, UNITS)]),
@@ -140,6 +150,10 @@
         copy.start()
         loading.append(copy)
 
+    loading[0].wait()
+    partial_ref[...] = jnp.dot(
+        read_ref[...], w_output[...], preferred_element_type=F32
+    ).astype(BF16)
     pl.semaphore_wait(barrier, 1 + RING - 1 + PLANE - 1)
 
     pending = []
@@ -152,8 +166,8 @@
     row = jnp.zeros((1, 128), F32)
     for i in range(ROWS):
         for k in range(2):
-            hit = lane == x * (ROWS * EXPERTS) + i * EXPERTS + ids_ref[k, i]
-            row = row + jnp.where(hit, weights_ref[k, i], 0.0)
+            hit = lane == x * (ROWS * EXPERTS) + i * EXPERTS + ids_ref[k : k + 1, i : i + 1]
+            row = row + jnp.where(hit, weights_ref[k : k + 1, i : i + 1], 0.0)
     weight_row[...] = row
     for d in range(1, RING):
         q = place * RING + lax.rem(x + d, RING)
@@ -208,7 +222,7 @@
         block = gathered.at[core, pl.ds(pl.multiple_of(came * BLOCK, BLOCK), BLOCK)]
         shared.append(send(block, block, share_send.at[i], share_recv.at[i], chip, other))
 
-    for copy in loading:
+    for copy in loading[1:]:
         copy.wait()
     pair[1].wait_recv()
     for half in range(2):
@@ -286,17 +300,187 @@
         b.wait_send()
 
 
-def ffn(tokens, partial, ffn_gain, ids, weights, scale, gate, up, down, dense_gate, dense_up, dense_down):
+def cell_kernel(
+    tokens_hbm,
+    gain_hbm,
+    w_gates_hbm,
+    w_forget_hbm,
+    bias_hbm,
+    stabilizer_hbm,
+    normalizer_hbm,
+    query_hbm,
+    key_hbm,
+    value_hbm,
+    memory_hbm,
+    read_ref,
+    new_memory_hbm,
+    new_normalizer_ref,
+    new_stabilizer_ref,
+    tokens,
+    gain,
+    w_gates,
+    w_forget,
+    bias,
+    stabilizer,
+    normalizer,
+    w_mixer,
+    memory,
+    turned,
+    load_sem,
+    store_sem,
+):
+    loads = [
+        (tokens_hbm, tokens),
+        (gain_hbm, gain),
+        (query_hbm, w_mixer.at[0]),
+        (w_gates_hbm, w_gates),
+        (w_forget_hbm, w_forget),
+        (bias_hbm, bias),
+        (stabilizer_hbm, stabilizer),
+        (normalizer_hbm, normalizer),
+        (key_hbm, w_mixer.at[1]),
+        (value_hbm, w_mixer.at[2]),
+        *[(memory_hbm.at[i], memory.at[i]) for i in range(PAIRS)],
+    ]
+    loading = []
+    for i, (src, dst) in enumerate(loads):
+        copy = pltpu.make_async_copy(src, dst, load_sem.at[i])
+        copy.start()
+        loading.append(copy)
+    loading[0].wait()
+    loading[1].wait()
+    normed = normalize(tokens[...], gain[...])
+
+    def projected(i, at):
+        loading[at].wait()
+        return jnp.dot(normed, w_mixer[i], preferred_element_type=F32).astype(BF16).astype(F32)
+
+    query = projected(0, 2)
+    for i in range(3, 8):
+        loading[i].wait()
+    nt = (((1,), (1,)), ((), ()))
+    in_gates = lax.dot_general(w_gates[...], normed, nt, preferred_element_type=F32)
+    forgets = lax.dot_general(w_forget[...], normed, nt, preferred_element_type=F32)
+    carries, admits, floors = [], [], []
+    for h in range(HEADS):
+        in_gate = in_gates[h : h + 1, :]
+        forget_log = jax.nn.log_sigmoid(forgets[h : h + 1, :] + bias[:, h : h + 1])
+        held = forget_log + stabilizer[h : h + 1, :]
+        new_stabilizer = jnp.maximum(held, in_gate)
+        new_stabilizer_ref[h : h + 1, :] = new_stabilizer
+        carries.append(jnp.exp(held - new_stabilizer))
+        admits.append(jnp.exp(in_gate - new_stabilizer))
+        floors.append(jnp.exp(-new_stabilizer))
+    key = projected(1, 8) * HEAD_SIZE ** (-0.5)
+    turned[...] = jnp.concatenate([query, key], axis=0).T
+    value = projected(2, 9)
+    storing = []
+    reads = [[None] * HEADS for _ in range(ROWS)]
+    for t in range(ROWS):
+        for h in range(HEADS):
+            pair = t * HEADS + h
+            part = slice(h * HEAD_SIZE, (h + 1) * HEAD_SIZE)
+            carry = carries[h][:, t : t + 1]
+            admit = admits[h][:, t : t + 1]
+            updated = carry * normalizer[t, h : h + 1, :] + admit * key[t : t + 1, part]
+            new_normalizer_ref[t, h : h + 1, :] = updated
+            denom = jnp.sum(updated * query[t : t + 1, part], axis=1, keepdims=True)
+            bound = jnp.maximum(jnp.abs(denom), floors[h][:, t : t + 1])
+            values = admit * value[t : t + 1, part]
+            loading[10 + pair].wait()
+
+            def step(c, total, pair=pair, h=h, t=t, carry=carry, values=values):
+                at = pl.multiple_of(c * CHUNK, CHUNK)
+                sides = turned[pl.ds(pl.multiple_of(h * HEAD_SIZE + at, CHUNK), CHUNK), :]
+                q, k = sides[:, t : t + 1], sides[:, ROWS + t : ROWS + t + 1]
+                new = carry * memory[pair, pl.ds(at, CHUNK), :] + k * values
+                memory[pair, pl.ds(at, CHUNK), :] = new
+                return total + jnp.sum((q * new).reshape(CHUNK // 8, 8, HEAD_SIZE), axis=0)
+
+            total = lax.fori_loop(
+                0, HEAD_SIZE // CHUNK, step, jnp.zeros((8, HEAD_SIZE), F32)
+            )
+            reads[t][h] = jnp.sum(total, axis=0, keepdims=True) / bound
+            copy = pltpu.make_async_copy(
+                memory.at[pair], new_memory_hbm.at[pair], store_sem.at[pair]
+            )
+            copy.start()
+            storing.append(copy)
+    rows = [jnp.concatenate(r, axis=1) for r in reads]
+    read_ref[...] = jnp.concatenate(rows, axis=0).astype(BF16)
+    for copy in storing:
+        copy.wait()
+
+
+def cell_step(
+    tokens,
+    mixer_gain,
+    w_input_gate,
+    w_forget_gate,
+    forget_bias,
+    stabilizer,
+    normalizer,
+    w_query,
+    w_key,
+    w_value,
+    memory,
+):
     vmem = pl.BlockSpec(memory_space=pltpu.VMEM)
-    smem = pl.BlockSpec(memory_space=pltpu.SMEM)
-    hbm = pl.BlockSpec(memory_space=pl.ANY)
+    hbm = pl.BlockSpec(memory_space=pltpu.HBM)
+    operands = (
+        tokens,
+        mixer_gain.reshape(1, WIDTH),
+        w_input_gate.T,
+        w_forget_gate.T,
+        forget_bias.reshape(1, HEADS),
+        stabilizer.T,
+        normalizer,
+        w_query,
+        w_key,
+        w_value,
+        memory.reshape(PAIRS, HEAD_SIZE, HEAD_SIZE),
+    )
+    read, new_memory, new_normalizer, new_stabilizer = pl.pallas_call(
+        cell_kernel,
+        out_shape=[
+            jax.ShapeDtypeStruct((ROWS, WIDTH), BF16),
+            pltpu.HBM((PAIRS, HEAD_SIZE, HEAD_SIZE), F32),
+            jax.ShapeDtypeStruct((ROWS, HEADS, HEAD_SIZE), F32),
+            jax.ShapeDtypeStruct((HEADS, ROWS), F32),
+        ],
+        in_specs=[hbm] * len(operands),
+        out_specs=[vmem, hbm, vmem, vmem],
+        scratch_shapes=[
+            pltpu.VMEM((ROWS, WIDTH), BF16),
+            pltpu.VMEM((1, WIDTH), F32),
+            pltpu.VMEM((HEADS, WIDTH), BF16),
+            pltpu.VMEM((HEADS, WIDTH), BF16),
+            pltpu.VMEM((1, HEADS), F32),
+            pltpu.VMEM((HEADS, ROWS), F32),
+            pltpu.VMEM((ROWS, HEADS, HEAD_SIZE), F32),
+            pltpu.VMEM((3, WIDTH, WIDTH), BF16),
+            pltpu.VMEM((PAIRS, HEAD_SIZE, HEAD_SIZE), F32),
+            pltpu.VMEM((WIDTH, 8), F32),
+            pltpu.SemaphoreType.DMA((10 + PAIRS,)),
+            pltpu.SemaphoreType.DMA((PAIRS,)),
+        ],
+        compiler_params=pltpu.CompilerParams(vmem_limit_bytes=K1_VMEM),
+    )(*[pltpu.with_memory_space_constraint(a, pltpu.HBM) for a in operands])
+    return read, new_memory.reshape(memory.shape), new_normalizer, new_stabilizer.T
+
+
+def ffn(tokens, read, ffn_gain, ids, weights, scale, w_output, gate, up, down, dense_gate, dense_up, dense_down):
+    vmem = pl.BlockSpec(memory_space=pltpu.VMEM)
+    hbm = pl.BlockSpec(memory_space=pltpu.HBM)
     dma = pltpu.SemaphoreType.DMA
     return pl.pallas_call(
         ffn_kernel,
         out_shape=jax.ShapeDtypeStruct((ROWS, HALF), BF16),
-        in_specs=[vmem, vmem, vmem, smem, smem, vmem] + [hbm] * 6,
+        in_specs=[vmem] * 6 + [hbm] * 7,
         out_specs=vmem,
         scratch_shapes=[
+            pltpu.VMEM((WIDTH, WIDTH), BF16),
+            pltpu.VMEM((ROWS, WIDTH), BF16),
             pltpu.VMEM((ROWS, WIDTH), BF16),
             pltpu.VMEM((2, 1, HALF), F32),
             pltpu.VMEM((2, ROWS, HALF), F32),
@@ -315,7 +499,7 @@
             pltpu.VMEM((PLANE, BLOCK, HALF), BF16),
             pltpu.VMEM((RING, ROWS, HALF), BF16),
             pltpu.VMEM((RING, ROWS, HALF), BF16),
-            dma((8,)),
+            dma((9,)),
             dma((2,)),
             dma((2,)),
             dma((2, RING)),
@@ -332,28 +516,20 @@
             dma((RING,)),
         ],
         compiler_params=pltpu.CompilerParams(
-            collective_id=0, has_side_effects=True, vmem_limit_bytes=32 * 2**20
+            collective_id=0, has_side_effects=True, vmem_limit_bytes=K2_VMEM
         ),
-    )(tokens, partial, ffn_gain, ids, weights, scale, gate, up, down, dense_gate, dense_up, dense_down)
-
-
-def cell_step(
-    query_heads, key_heads, value_heads, in_gate, forget_log, memory, normalizer, stabilizer
-):
-    new_stabilizer = jnp.maximum(forget_log + stabilizer, in_gate)
-    carry = jnp.exp(forget_log + stabilizer - new_stabilizer)
-    admit = jnp.exp(in_gate - new_stabilizer)
-    scaled_key = admit[..., None] * key_heads
-    new_memory = (
-        carry[..., None, None] * memory + scaled_key[..., :, None] * value_heads[..., None, :]
+    )(
+        tokens,
+        read,
+        ffn_gain,
+        ids,
+        weights,
+        scale,
+        *[
+            pltpu.with_memory_space_constraint(w, pltpu.HBM)
+            for w in (w_output, gate, up, down, dense_gate, dense_up, dense_down)
+        ],
     )
-    new_normalizer = carry[..., None] * normalizer + scaled_key
-    numer = jnp.einsum(
-        "...hd,...hde->...he", query_heads, new_memory, precision=lax.Precision.HIGHEST
-    )
-    denom = jnp.sum(new_normalizer * query_heads, axis=-1)
-    bound = jnp.maximum(jnp.abs(denom), jnp.exp(-new_stabilizer))
-    return (numer / bound[..., None], new_memory, new_normalizer, new_stabilizer)
 
 
 def shards(
@@ -380,34 +556,27 @@
     dense_down_w,
     dense_scale,
 ):
-    local_rows = tokens.shape[0]
-    local_heads = memory.shape[1]
-    head_size = memory.shape[2]
-    width = tokens.shape[1]
-    normed = normalize(tokens, mixer_gain)
-    query = jnp.dot(normed, w_query, preferred_element_type=jnp.float32).astype(jnp.bfloat16)
-    key = jnp.dot(normed, w_key, preferred_element_type=jnp.float32).astype(jnp.bfloat16)
-    value = jnp.dot(normed, w_value, preferred_element_type=jnp.float32).astype(jnp.bfloat16)
-    in_gate = jnp.dot(normed, w_input_gate, preferred_element_type=jnp.float32)
-    forget_log = jax.nn.log_sigmoid(
-        jnp.dot(normed, w_forget_gate, preferred_element_type=jnp.float32) + forget_bias
+    read, new_memory, new_normalizer, new_stabilizer = cell_step(
+        tokens,
+        mixer_gain,
+        w_input_gate,
+        w_forget_gate,
+        forget_bias,
+        stabilizer,
+        normalizer,
+        w_query,
+        w_key,
+        w_value,
+        memory,
     )
-    shaped = (local_rows, local_heads, head_size)
-    query_heads = query.astype(jnp.float32).reshape(shaped)
-    key_heads = key.astype(jnp.float32).reshape(shaped) * head_size ** (-0.5)
-    value_heads = value.astype(jnp.float32).reshape(shaped)
-    read, new_memory, new_normalizer, new_stabilizer = cell_step(
-        query_heads, key_heads, value_heads, in_gate, forget_log, memory, normalizer, stabilizer
-    )
-    read = read.reshape(local_rows, local_heads * head_size).astype(jnp.bfloat16)
-    partial_value = jnp.dot(read, w_output, preferred_element_type=jnp.float32)
     output = ffn(
         tokens,
-        partial_value.astype(jnp.bfloat16),
-        ffn_gain.reshape(1, width),
+        read,
+        ffn_gain.reshape(1, WIDTH),
         route_ids.T,
         route_weights.T,
-        dense_scale.reshape(1, -1),
+        dense_scale.reshape(1, HALF),
+        w_output,
         expert_gate[0].T,
         expert_up[0].T,
         expert_down[0],

time: 67.3 us -> 46.4 us (0.69)
  matrix products: 14.7 us -> 0 us
  Pallas kernels: 31.8 us -> 45 us
  other arithmetic: 11.3 us -> 0 us
  local copies, waits for them, and re-layouts: 8.11 us -> 0.62 us
    dot_general x7 -> x0, matrix products: 14.7 us -> none  [the longest x1 6.73 us: cell_step(): jnp.einsum('...hd,...hde->...he', query_heads, new_memory, precision=lax....]
    pallas_call x0 -> x1, Pallas kernels: none -> 13.7 us  [cell_step(): pl.pallas_call(cell_kernel, out_shape=[jax.ShapeDtypeStruct((ROWS, WIDTH)...]
    add x1 -> x0, other arithmetic: 6.12 us -> none  [cell_step(): carry[..., None, None] * memory]
    unnamed x30 -> x11, local copies, waits for them, and re-layouts: 5.07 us -> 0.62 us
    reduce_sum x2 -> x0, other arithmetic: 2.23 us -> none  [the longest x1 1.27 us: cell_step(): denom = jnp.sum(new_normalizer * query_heads, axis=-1)]
    reduce_sum x1 -> x0, local copies, waits for them, and re-layouts: 1.44 us -> none  [cell_step(): denom = jnp.sum(new_normalizer * query_heads, axis=-1)]
    max x1 -> x0, local copies, waits for them, and re-layouts: 1.32 us -> none  [cell_step(): bound = jnp.maximum(jnp.abs(denom), jnp.exp(-new_stabilizer))]
    max x1 -> x0, other arithmetic: 1.26 us -> none  [cell_step(): bound = jnp.maximum(jnp.abs(denom), jnp.exp(-new_stabilizer))]
where the time goes in v2:
time: 46.4 us; the launch traced here: 46.3 us
  Pallas kernels  45 us (97%)
  between operations  0.73 us (2%)
  local copies, waits for them, and re-layouts  0.62 us (1%)
    pallas_call x1, Pallas kernels, ffn(): pl.pallas_call(ffn_kernel, out_shape=jax.ShapeDtypeStruct((ROWS, HALF), B...  31.3 us
    pallas_call x1, Pallas kernels, cell_step(): pl.pallas_call(cell_kernel, out_shape=[jax.ShapeDtypeStruct((ROWS, WIDTH)...  13.7 us

profile of v2, /device:TPU:0, one launch (start us, length us, event | category | flops | bytes accessed | tf_op | source)
XLA Modules:
  0.0 46.3 jit_solution(257306561113254797)
XLA Ops:
  0.6 0.0 copy-start
  0.6 0.0 copy-start.1
  0.7 0.0 copy-start.2
  0.7 0.0 copy-start.3
  0.7 0.0 copy-start.4
  0.7 13.7 %shard_map.237 = (bf16[4,1024]{1,0:T(4,128)(2,1)S(1)}, f32[8,512,512]{2,1,0:T(8,128)}, f32[4,2,512]{2,1,0:T(2,128)}, f32[2,4]{1,0:T(2,128)}) custom-call(bf16[4,1024]{1,0:T(4,128)(2,1)} %tokens_ref.1, f32[1,1024]{1,0:T(1,128)} %bitcast.31, bf16[2,1024]{1,0:T(2,128)(2,1)} %bitcast.32, bf16[2,1024]{1,0:T(2,128)(2,1)} %bitcast.33, f32[1,2]{1,0:T(1,128)} %bitcast.35, ...), custom_call_target="tpu_custom_call" | custom-call | tf_op jit(solution)/shard_map/pallas_call | solution.py:443
  14.4 0.0 copy-done
  14.4 0.0 copy-done.1
  14.4 0.0 copy-done.2
  14.4 0.0 copy-done.3
  14.4 0.0 copy-done.4
  14.4 31.3 %shard_map.238 = bf16[4,512]{1,0:T(4,128)(2,1)S(1)} custom-call(bf16[4,1024]{1,0:T(4,128)(2,1)S(1)} %copy-done, bf16[4,1024]{1,0:T(4,128)(2,1)S(1)} %get-tuple-element.8.read_ref, f32[1,1024]{1,0:T(1,128)S(1)} %bitcast.21, s32[2,4]{1,0:T(2,128)S(1)} %bitcast.23, f32[2,4]{1,0:T(2,128)S(1)} %bitcast.24, f32[1,512]{1,0:T(1,128)S(1)} %bitcast.22, ...), custom_call_target="tpu_custom_call" | custom-call | tf_op jit(solution)/shard_map/pallas_call | solution.py:476
  45.7 0.6 %copy.27 = bf16[4,512]{1,0:T(4,128)(2,1)} copy(bf16[4,512]{1,0:T(4,128)(2,1)S(1)} %shard_map.238) | data formatting | bytes 8192
Async XLA Ops:
  0.6 13.7 %copy-start = (bf16[4,1024]{1,0:T(4,128)(2,1)S(1)}, bf16[4,1024]{1,0:T(4,128)(2,1)}, u32[]{:S(2)}) copy-start(bf16[4,1024]{1,0:T(4,128)(2,1)} %tokens_ref.1) | copy-start | bytes 24580
  0.6 13.7 %copy-start.1 = (f32[1024]{0:T(1024)S(1)}, f32[1024]{0:T(1024)}, u32[]{:S(2)}) copy-start(f32[1024]{0:T(1024)} %param.34) | copy-start | bytes 12292
  0.7 13.7 %copy-start.2 = (f32[512]{0:T(512)S(1)}, f32[512]{0:T(512)}, u32[]{:S(2)}) copy-start(f32[512]{0:T(512)} %param.43) | copy-start | bytes 6148
  0.7 13.7 %copy-start.3 = (s32[4,2]{0,1:T(2,128)S(1)}, s32[4,2]{0,1:T(2,128)}, u32[]{:S(2)}) copy-start(s32[4,2]{0,1:T(2,128)} %param.35) | copy-start | bytes 100
  0.7 13.7 %copy-start.4 = (f32[4,2]{0,1:T(2,128)S(1)}, f32[4,2]{0,1:T(2,128)}, u32[]{:S(2)}) copy-start(f32[4,2]{0,1:T(2,128)} %param.36) | copy-start | bytes 100
